TPU v7x, 32 devices: a whole 2x2x4 slice. The times are simulated.
32 devices in a mesh: rep: 2 (over x), fs: 4 (over z), tp: 4 (over y, core).
Axes of the slice: x: 2, y: 2, z: 4, core: 2. Of those that a mesh axis runs over, the one named last changes fastest.
Arguments:
- tokens: bfloat16 [8, 1024, 2048], P(('rep', 'fs')), may hold values from -6 to 6
- mix_gain: bfloat16 [2048], replicated, may hold values from 0.099609375 to 1.8984375
- value_weight: bfloat16 [2048, 1024], P('fs', 'tp'), may hold values from -0.125 to 0.125
- gate_weight: bfloat16 [2048, 1024], P('fs', 'tp'), may hold values from -0.125 to 0.125
- mix_taps: bfloat16 [31, 1024], P(None, 'tp'), may hold values from -1 to 1
- head_gain: bfloat16 [1024], P('tp'), may hold values from 0.099609375 to 1.8984375
- out_weight: bfloat16 [1024, 2048], P('fs', 'tp'), may hold values from -0.1875 to 0.1875
- ffn_gain: bfloat16 [2048], replicated, may hold values from 0.099609375 to 1.8984375
- ffgate_weight: bfloat16 [2048, 6144], P('fs', 'tp'), may hold values from -0.125 to 0.125
- up_weight: bfloat16 [2048, 6144], P('fs', 'tp'), may hold values from -0.125 to 0.125
- ff_taps: bfloat16 [3, 6144], P(None, 'tp'), may hold values from -3.5 to 3.5
- down_weight: bfloat16 [2048, 6144], P('fs', 'tp'), may hold values from -0.078125 to 0.078125
Outputs:
- layer_out: bfloat16 [8, 1024, 2048], P(('rep', 'fs'), 'tp')
All inputs are finite; a program needn't handle non-finite values.
Results may differ from a plain program's by a relative error of at most 0.01.
Values may be sent and summed in bfloat16 or wider, within the bound.
A program may use at most 128 MiB of HBM per device.

v0:
```python
import functools

import jax
import jax.numpy as jnp
from jax import lax
from jax.experimental import pallas as pl
from jax.experimental.pallas import tpu as pltpu
from jax.sharding import PartitionSpec as P

HEAD = 128
MESH = pl.DeviceIdType.MESH
F32 = jnp.float32
BF16 = jnp.bfloat16
norm_floor = 0.01


def row_norm(floats_in, scales):
    floats = floats_in.astype(F32)
    scaled = floats * lax.rsqrt(jnp.mean(floats * floats, axis=-1, keepdims=True) + norm_floor)
    return (scaled * scales.astype(F32)).astype(BF16)


def causal_conv(signal, kernel_taps):
    reach = kernel_taps.shape[0]
    length = signal.shape[0]
    padded = jnp.pad(signal, ((reach - 1, 0), (0, 0)))
    summed = padded[0:length] * kernel_taps[0]
    for offset in range(1, reach):
        summed = summed + padded[offset : offset + length] * kernel_taps[offset]
    return summed


def head_norm(signal, scales):
    heads = []
    for start in range(0, signal.shape[1], HEAD):
        part = signal[:, start : start + HEAD]
        centre = part - jnp.mean(part, axis=-1, keepdims=True)
        spread = jnp.mean(centre * centre, axis=-1, keepdims=True)
        gain = scales[start : start + HEAD].astype(F32)
        heads.append(jax.nn.silu(centre * lax.rsqrt(spread + norm_floor) * gain))
    return jnp.concatenate(heads, axis=1).astype(BF16)


def plain(
    tokens,
    mix_gain,
    value_weight,
    gate_weight,
    mix_taps,
    head_gain,
    out_weight,
    ffn_gain,
    ffgate_weight,
    up_weight,
    ff_taps,
    down_weight,
):
    def rows_of(shard):
        return lax.all_gather(shard, "fs", axis=0, tiled=True)

    sequence = tokens[0]
    width = value_weight.shape[1]
    pair_full = rows_of(jnp.concatenate([value_weight, gate_weight], axis=1))
    out_full = rows_of(out_weight)
    normed = row_norm(sequence, mix_gain)
    both = jnp.dot(normed, pair_full, preferred_element_type=F32)
    glu_out = both[:, :width] * jax.nn.sigmoid(both[:, width:])
    mixed_pos = causal_conv(glu_out, mix_taps.astype(F32))
    head_out = head_norm(mixed_pos, head_gain)
    out_cols = out_full.shape[1]
    all_heads = lax.all_gather(head_out, "tp", axis=1, tiled=True)
    own_cols = lax.dynamic_slice_in_dim(sequence, lax.axis_index("tp") * out_cols, out_cols, 1)
    mixer_sum = jnp.dot(all_heads, out_full, preferred_element_type=F32)
    hidden_cols = (own_cols.astype(F32) + mixer_sum).astype(BF16)
    full_rows = lax.all_gather(hidden_cols, "tp", axis=1, tiled=True)
    normed_ffn = row_norm(full_rows, ffn_gain)
    ffgate = jnp.dot(normed_ffn, rows_of(ffgate_weight), preferred_element_type=F32)
    gated = jax.nn.silu(causal_conv(ffgate, ff_taps.astype(F32)))
    ff_up = jnp.dot(normed_ffn, rows_of(up_weight), preferred_element_type=F32)
    product = (gated * ff_up).astype(BF16)
    own_count = sequence.shape[0] // lax.axis_size("tp")
    own_rows = lax.dynamic_slice_in_dim(full_rows, lax.axis_index("tp") * own_count, own_count, 0)
    partial = lax.dot_general(
        product, rows_of(down_weight), (((1,), (1,)), ((), ())), preferred_element_type=F32
    )
    result = lax.psum_scatter(partial.astype(BF16), "tp", scatter_dimension=0, tiled=True)
    return (own_rows.astype(F32) + result.astype(F32)).astype(BF16)[None]


def kernel(
    tokens,
    mix_gain,
    value_w,
    gate_w,
    mix_taps,
    head_gain,
    out_w,
    ffn_gain,
    ffgate_w,
    up_w,
    ff_taps,
    down_w,
    out,
    tok,
    normed,
    wpair,
    wout,
    glu,
    heads,
    hid,
    xc,
    wg,
    wu,
    wd,
    gbuf,
    ubuf,
    prod,
    part,
    rs1,
    sum1,
    rs2,
    sum2,
    rs3,
    loc,
    tsem,
    zs,
    zr,
    xs,
    xr,
    hs,
    hr,
    es,
    er,
    qs,
    qr,
):
    r, f, t = lax.axis_index("rep"), lax.axis_index("fs"), lax.axis_index("tp")
    y, c = t // 2, t % 2
    zl, zh = f % 2, f // 2
    fp = f + 1 - 2 * zl
    sib, ynb = t + 1 - 2 * c, (t + 2) % 4
    far = (sib + 2) % 4
    to_x, to_z, to_sib, to_y = {"rep": 1 - r}, {"fs": fp}, {"tp": sib}, {"tp": ynb}

    length, width = tok.shape
    chunk = length // 4
    cw = value_w.shape[1]
    ow = out_w.shape[1]
    hw = wg.shape[1]
    feat = down_w.shape[0] // 2

    def remote(src, dst, ss, rs, where):
        return pltpu.make_async_remote_copy(
            src_ref=src, dst_ref=dst, send_sem=ss, recv_sem=rs, device_id=where, device_id_type=MESH
        )

    barrier = pltpu.get_barrier_semaphore()
    for peer in (to_x, to_sib, to_y, {"fs": (f + 1) % 4}, {"fs": (f + 2) % 4}, {"fs": (f + 3) % 4}):
        pl.semaphore_signal(barrier, inc=1, device_id=peer, device_id_type=MESH)

    def rows(j):
        return pl.ds(pl.multiple_of(j * chunk, chunk), chunk)

    def tok_copy(j):
        return pltpu.make_async_copy(tokens.at[0, rows(j), :], tok.at[rows(j), :], tsem.at[j])

    for j in range(4):
        tok_copy(j).start()

    mats = (
        (value_w, wpair, 0, False),
        (gate_w, wpair, cw, False),
        (out_w, wout, 0, False),
        (ffgate_w, wg, 0, True),
        (up_w, wu, 0, True),
        (down_w, wd, 0, True),
    )

    def src_of(m, row, count, parity):
        w, dst, col, halves = mats[m]
        if halves:
            return w.at[pl.ds(row, count), pl.ds(pl.multiple_of(parity * hw, 128), hw)]
        return w.at[pl.ds(row, count), :]

    def dst_of(m, row, count):
        w, dst, col, halves = mats[m]
        size = hw if halves else w.shape[1]
        return dst.at[pl.ds(row, count), pl.ds(col, size)]

    def piece(m, owner, half):
        n = mats[m][0].shape[0]
        return dst_of(m, pl.multiple_of(owner * n + half * (n // 2), n // 2), n // 2)

    def own_copy(m):
        n = mats[m][0].shape[0]
        return pltpu.make_async_copy(
            src_of(m, 0, n, zl), dst_of(m, pl.multiple_of(f * n, n), n), loc.at[m]
        )

    def z_copy(m, target):
        n = mats[m][0].shape[0]
        return remote(
            src_of(m, pl.multiple_of(r * (n // 2), n // 2), n // 2, target % 2),
            piece(m, f, r),
            zs.at[m, target],
            zr.at[m, f],
            {"fs": target},
        )

    def z_arrived(m, owner):
        n = mats[m][0].shape[0]
        remote(piece(m, owner, r), piece(m, owner, r), zs.at[m, owner], zr.at[m, owner], to_x).wait_recv()

    def x_copy(m, owner):
        return remote(piece(m, owner, r), piece(m, owner, r), xs.at[m, owner], xr.at[m, owner], to_x)

    def x_arrived(m, owner):
        remote(
            piece(m, owner, 1 - r), piece(m, owner, 1 - r), xs.at[m, owner], xr.at[m, owner], to_x
        ).wait_recv()

    def others(fn):
        def step(k, carry):
            fn((f + k) % 4)
            return carry

        lax.fori_loop(1, 4, step, 0)

    for m in range(6):
        own_copy(m).start()
    pl.semaphore_wait(barrier, 6)

    def send_weights(*ms):
        def one(target):
            for m in ms:
                z_copy(m, target).start()

        others(one)

    def pass_on(*ms):
        def one(owner):
            for m in ms:
                z_arrived(m, owner)
                x_copy(m, owner).start()

        others(one)

    def collect(*ms):
        def one(owner):
            for m in ms:
                x_arrived(m, owner)

        others(one)
        for m in ms:
            own_copy(m).wait()

    send_weights(0, 1)
    send_weights(2)
    send_weights(3)

    def norm_rows(src, dst, gain_ref, count):
        gain = gain_ref[...].astype(F32)

        def step(i, carry):
            at = pl.ds(pl.multiple_of(i * 16, 16), 16)
            v = src[at, :].astype(F32)
            s = lax.rsqrt(jnp.mean(v * v, axis=-1, keepdims=True) + norm_floor)
            dst[at, :] = (v * s * gain).astype(BF16)
            return carry

        lax.fori_loop(0, count // 16, step, 0, unroll=4)

    glu[pl.ds(0, 32), :] = jnp.zeros((32, cw), F32)
    for j in range(4):
        tok_copy(j).wait()
    norm_rows(tok, normed, mix_gain, length)

    pass_on(0, 1)
    collect(0, 1)

    def head_cols(who):
        return pl.ds(pl.multiple_of(who * cw, 128), cw)

    def head_send(kind, j, who, where):
        block = heads.at[rows(j), head_cols(who)]
        return remote(block, block, hs.at[kind, j], hr.at[kind, j], where)

    def head_wait(kind, j, who):
        block = heads.at[rows(j), head_cols(who)]
        remote(block, block, hs.at[kind, j], hr.at[kind, j], to_sib).wait_recv()

    reach = mix_taps.shape[0]
    sub = 32

    def mix_chunk(j, carry):
        both = jnp.dot(normed[rows(j), :], wpair[...], preferred_element_type=F32)
        glu[pl.ds(pl.multiple_of(j * chunk + 32, 32), chunk), :] = both[:, :cw] * jax.nn.sigmoid(both[:, cw:])

        def conv_step(i, inner):
            base = pl.multiple_of(j * chunk + i * sub, sub)
            window = glu[pl.ds(base, sub + 32), :]
            acc = None
            for k in range(reach):
                o = 32 - (reach - 1) + k
                term = window[o : o + sub, :] * mix_taps[k : k + 1, :].astype(F32)
                acc = term if acc is None else acc + term
            parts = []
            for h in range(0, cw, HEAD):
                v = acc[:, h : h + HEAD]
                v = v - jnp.mean(v, axis=-1, keepdims=True)
                s = lax.rsqrt(jnp.mean(v * v, axis=-1, keepdims=True) + norm_floor)
                v = v * s * head_gain[:, h : h + HEAD].astype(F32)
                parts.append(v * jax.nn.sigmoid(v))
            heads[pl.ds(base, sub), head_cols(t)] = jnp.concatenate(parts, axis=1).astype(BF16)
            return inner

        lax.fori_loop(0, chunk // sub, conv_step, 0)
        head_send(0, j, t, to_sib).start()
        head_send(1, j, t, to_y).start()
        return carry

    lax.fori_loop(0, 4, mix_chunk, 0)
    pass_on(2)

    def heads_on(j, carry):
        head_wait(1, j, ynb)
        head_send(2, j, ynb, to_sib).start()
        return carry

    lax.fori_loop(0, 4, heads_on, 0)
    collect(2)

    def hid_block(seq, j, who):
        return hid.at[seq, rows(j), pl.ds(pl.multiple_of(who * ow, 128), ow)]

    def hid_send(kind, j, seq, who, where):
        block = hid_block(seq, j, who)
        return remote(block, block, es.at[kind, j], er.at[kind, j], where)

    def hid_wait(kind, j, seq, who):
        block = hid_block(seq, j, who)
        remote(block, block, es.at[kind, j], er.at[kind, j], to_sib).wait_recv()

    def out_chunk(j, carry):
        head_wait(0, j, sib)
        head_wait(2, j, far)
        own = tok[rows(j), pl.ds(pl.multiple_of(t * ow, 128), ow)].astype(F32)
        total = own + jnp.dot(heads[rows(j), :], wout[...], preferred_element_type=F32)
        hid[zl, rows(j), pl.ds(pl.multiple_of(t * ow, 128), ow)] = total.astype(BF16)
        hid_send(0, j, zl, t, to_sib).start()
        hid_send(1, j, zl, t, to_y).start()
        hid_send(2, j, zl, t, to_z).start()
        return carry

    lax.fori_loop(0, 4, out_chunk, 0)
    send_weights(4)
    send_weights(5)

    def hid_on(j, carry):
        hid_wait(1, j, zl, ynb)
        hid_send(3, j, zl, ynb, to_sib).start()
        hid_wait(2, j, 1 - zl, t)
        hid_send(4, j, 1 - zl, t, to_sib).start()
        hid_send(5, j, 1 - zl, t, to_y).start()
        return carry

    lax.fori_loop(0, 4, hid_on, 0)
    pass_on(3)

    def hid_on2(j, carry):
        hid_wait(5, j, 1 - zl, ynb)
        hid_send(6, j, 1 - zl, ynb, to_sib).start()
        return carry

    lax.fori_loop(0, 4, hid_on2, 0)
    pass_on(4)
    collect(3, 4)

    freach = ff_taps.shape[0]
    asub = 32

    def ffn_chunk(i, carry):
        first = i < 4
        j = i % 4
        seq = jnp.where(first, zl, 1 - zl)

        @pl.when(first)
        def _():
            hid_wait(0, j, zl, sib)
            hid_wait(3, j, zl, far)

        @pl.when(jnp.logical_not(first))
        def _():
            hid_wait(4, j, 1 - zl, sib)
            hid_wait(6, j, 1 - zl, far)

        norm_rows(hid.at[seq, rows(j), :], xc, ffn_gain, chunk)
        keep = jnp.where(j == 0, 0.0, 1.0)
        gbuf[pl.ds(0, 8), :] = gbuf[pl.ds(chunk, 8), :]

        @pl.when(j == 0)
        def _():
            gbuf[pl.ds(0, 8), :] = jnp.zeros((8, hw), F32)

        gbuf[pl.ds(8, chunk), :] = jnp.dot(xc[...], wg[...], preferred_element_type=F32)
        ubuf[...] = jnp.dot(xc[...], wu[...], preferred_element_type=F32)

        def act(a, inner):
            base = pl.multiple_of(a * asub, asub)
            window = gbuf[pl.ds(base, asub + 8), :]
            acc = None
            for k in range(freach):
                o = 8 - (freach - 1) + k
                term = window[o : o + asub, :] * ff_taps[k : k + 1, :].astype(F32)
                acc = term if acc is None else acc + term
            v = acc * jax.nn.sigmoid(acc) * ubuf[pl.ds(base, asub), :]
            prod[pl.ds(pl.multiple_of(seq * length + j * chunk + base, asub), asub), :] = v.astype(BF16)
            return inner

        lax.fori_loop(0, chunk // asub, act, 0)
        return carry

    lax.fori_loop(0, 8, ffn_chunk, 0)

    own_copy(5).wait()
    blocks = 8

    def place(i):
        late = i // 4
        k = i % 4
        owner = jnp.where(late == 0, 2 * zh + k // 2, 2 * (1 - zh) + k % 2)
        flip = jnp.where(late == 0, k % 2, k // 2)
        half = jnp.where(flip == 0, r, 1 - r)
        return owner, flip, half

    def q1(i):
        return remote(part.at[i % 3, 1 - c], rs1.at[i], qs.at[0, i], qr.at[0, i], to_sib)

    def q2(i):
        return remote(sum1.at[i % 3, 1 - y], rs2.at[i], qs.at[1, i], qr.at[1, i], to_y)

    def q3(i):
        return remote(sum2.at[i % 3, 1 - zl], rs3.at[i], qs.at[2, i], qr.at[2, i], to_z)

    def turn(i, carry):
        @pl.when(i == 0)
        def _():
            z_arrived(5, fp)
            x_copy(5, fp).start()

        @pl.when((i == 2) | (i == 3))
        def _():
            owner = 2 * (1 - zh) + i % 2
            z_arrived(5, owner)
            x_copy(5, owner).start()

        @pl.when(i < blocks)
        def _():
            owner, flip, half = place(i)

            @pl.when((owner != f) & (flip == 1))
            def _():
                x_arrived(5, owner)

            @pl.when(i >= 3)
            def _():
                q1(i - 3).wait_send()

            at = pl.ds(pl.multiple_of(owner * 2 * feat + half * feat, feat), feat)

            def block_rows(b, inner):
                cc, yy, ss = b // 4, (b // 2) % 2, b % 2
                row = pl.multiple_of(ss * length + (2 * yy + cc) * chunk, chunk)
                part[i % 3, cc, yy, ss] = lax.dot_general(
                    prod[pl.ds(row, chunk), :],
                    wd[at, :],
                    (((1,), (1,)), ((), ())),
                    preferred_element_type=F32,
                ).astype(BF16)
                return inner

            lax.fori_loop(0, 8, block_rows, 0)
            q1(i).start()

        @pl.when((i >= 1) & (i <= blocks))
        def _():
            n = i - 1
            q1(n).wait_recv()

            @pl.when(n >= 3)
            def _():
                q2(n - 3).wait_send()

            sum1[n % 3] = (part[n % 3, c].astype(F32) + rs1[n].astype(F32)).astype(BF16)
            q2(n).start()

        @pl.when((i >= 2) & (i <= blocks + 1))
        def _():
            n = i - 2
            q2(n).wait_recv()

            @pl.when(n >= 3)
            def _():
                q3(n - 3).wait_send()

            sum2[n % 3] = (sum1[n % 3, y].astype(F32) + rs2[n].astype(F32)).astype(BF16)
            q3(n).start()

        @pl.when(i >= 3)
        def _():
            n = i - 3
            q3(n).wait_recv()
            owner, flip, half = place(n)
            cols = pl.ds(pl.multiple_of(owner * 2 * feat + half * feat, feat), feat)
            base = hid[zl, pl.ds(pl.multiple_of(t * chunk, chunk), chunk), cols].astype(F32)
            total = base + (sum2[n % 3, zl].astype(F32) + rs3[n].astype(F32))
            out[0, :, cols] = total.astype(BF16)

        return carry

    lax.fori_loop(0, blocks + 3, turn, 0)

    for n in range(blocks - 3, blocks):
        q1(n).wait_send()
        q2(n).wait_send()
        q3(n).wait_send()

    def drain(target):
        for m in range(6):
            z_copy(m, target).wait_send()
            x_copy(m, target).wait_send()

    others(drain)

    def drain_chunks(j, carry):
        head_send(0, j, t, to_sib).wait_send()
        head_send(1, j, t, to_y).wait_send()
        head_send(2, j, ynb, to_sib).wait_send()
        hid_send(0, j, zl, t, to_sib).wait_send()
        hid_send(1, j, zl, t, to_y).wait_send()
        hid_send(2, j, zl, t, to_z).wait_send()
        hid_send(3, j, zl, ynb, to_sib).wait_send()
        hid_send(4, j, 1 - zl, t, to_sib).wait_send()
        hid_send(5, j, 1 - zl, t, to_y).wait_send()
        hid_send(6, j, 1 - zl, ynb, to_sib).wait_send()
        return carry

    lax.fori_loop(0, 4, drain_chunks, 0)


def fused(*arrays):
    (tokens, mix_gain, value_w, gate_w, mix_taps, head_gain, out_w, ffn_gain, ffgate_w, up_w, ff_taps, down_w) = arrays
    _, length, width = tokens.shape
    fs = lax.axis_size("fs")
    cw, ow = value_w.shape[1], out_w.shape[1]
    hw = ffgate_w.shape[1] // 2
    chunk = length // 4
    feat = down_w.shape[0] // 2
    zl = lax.axis_index("fs") % 2
    taps = lax.dynamic_slice_in_dim(ff_taps, zl * hw, hw, 1)
    scratch = [
        pltpu.VMEM((length, width), BF16),
        pltpu.VMEM((length, width), BF16),
        pltpu.VMEM((fs * value_w.shape[0], 2 * cw), BF16),
        pltpu.VMEM((fs * out_w.shape[0], ow), BF16),
        pltpu.VMEM((length + 32, cw), F32),
        pltpu.VMEM((length, 4 * cw), BF16),
        pltpu.VMEM((2, length, width), BF16),
        pltpu.VMEM((chunk, width), BF16),
        pltpu.VMEM((fs * ffgate_w.shape[0], hw), BF16),
        pltpu.VMEM((fs * up_w.shape[0], hw), BF16),
        pltpu.VMEM((fs * down_w.shape[0], hw), BF16),
        pltpu.VMEM((chunk + 8, hw), F32),
        pltpu.VMEM((chunk, hw), F32),
        pltpu.VMEM((2 * length, hw), BF16),
        pltpu.VMEM((3, 2, 2, 2, chunk, feat), BF16),
        pltpu.VMEM((8, 2, 2, chunk, feat), BF16),
        pltpu.VMEM((3, 2, 2, chunk, feat), BF16),
        pltpu.VMEM((8, 2, chunk, feat), BF16),
        pltpu.VMEM((3, 2, chunk, feat), BF16),
        pltpu.VMEM((8, chunk, feat), BF16),
        pltpu.SemaphoreType.DMA((6,)),
        pltpu.SemaphoreType.DMA((4,)),
    ]
    scratch += [pltpu.SemaphoreType.DMA((6, 4))] * 4
    scratch += [pltpu.SemaphoreType.DMA((3, 4))] * 2
    scratch += [pltpu.SemaphoreType.DMA((7, 4))] * 2
    scratch += [pltpu.SemaphoreType.DMA((3, 8))] * 2
    anywhere = pl.BlockSpec(memory_space=pl.ANY)
    small = pl.BlockSpec(memory_space=pltpu.VMEM)
    return pl.pallas_call(
        kernel,
        out_shape=jax.ShapeDtypeStruct((1, chunk, width), BF16),
        in_specs=[anywhere, small, anywhere, anywhere, small, small, anywhere, small, anywhere, anywhere, small, anywhere],
        out_specs=small,
        scratch_shapes=scratch,
        compiler_params=pltpu.CompilerParams(
            collective_id=0, has_side_effects=True, vmem_limit_bytes=67043328
        ),
        name="layer",
    )(
        tokens,
        mix_gain[None],
        value_w,
        gate_w,
        mix_taps,
        head_gain[None],
        out_w,
        ffn_gain[None],
        ffgate_w,
        up_w,
        taps,
        down_w,
    )


def solution(mesh):
    placed = (
        P(("rep", "fs"), None, None),
        P(),
        P("fs", "tp"),
        P("fs", "tp"),
        P(None, "tp"),
        P("tp"),
        P("fs", "tp"),
        P(),
        P("fs", "tp"),
        P("fs", "tp"),
        P(None, "tp"),
        P("fs", "tp"),
    )
    shape = mesh.shape
    small = shape["rep"] == 2 and shape["fs"] == 4 and shape["tp"] == 4
    return jax.shard_map(
        fused if small else plain,
        mesh=mesh,
        in_specs=placed,
        out_specs=P(("rep", "fs"), "tp", None),
        check_vma=False,
    )
```

profile of v0, /device:TPU:0, one launch (start us, length us, event | category | flops | bytes accessed | tf_op | source)
XLA Modules:
  0.0 278.7 jit_solution(12446970757510284323)
XLA Ops:
  0.0 1.2 broadcast_in_dim.10.head_gain
  1.2 1.3 constant_dynamic-slice_fusion.ff_taps
  2.5 1.3 broadcast_in_dim.9.mix_gain
  3.8 1.3 broadcast_in_dim.11.ffn_gain
  5.1 271.3 %layer.1 = bf16[1,256,2048]{2,1,0:T(8,128)(2,1)} custom-call(bf16[1,1024,2048]{2,1,0:T(8,128)(2,1)} %tokens.1, bf16[1,2048]{1,0:T(2,128)(2,1)} %broadcast_in_dim.9.mix_gain, bf16[512,256]{1,0:T(8,128)(2,1)} %value_w.1, bf16[512,256]{1,0:T(8,128)(2,1)} %gate_w.1, bf16[31,256]{1,0:T(8,128)(2,1)} %mix_taps.1, bf16[1,256]{1,0:T(2,128)(2,1)} %broadcast_in_dim.10.head_gain, ...), custom_call_target="tpu_custom_call" | custom-call | tf_op jit(solution)/shard_map/layer/pallas_call | solution.py:591
  276.4 2.3 copy.14
where the time goes:
time: 279 us
  Pallas kernels  271 us (97%)
  local copies, waits for them, and re-layouts  7.39 us (3%)
    pallas_call x1, Pallas kernels, fused(): pl.pallas_call(kernel, out_shape=jax.ShapeDtypeStruct((1, chunk, width),...  271 us

commit v1 on v0

--- a/solution.py
+++ b/solution.py
@@ -109,6 +109,7 @@
     heads,
     hid,
     xc,
+    tapb,
     wg,
     wu,
     wd,
@@ -221,29 +222,89 @@
 
     def others(fn):
         def step(k, carry):
-            fn((f + k) % 4)
+            fn(jnp.where(k == 0, fp, jnp.where(k == 1, 2 - zh, 3 - 3 * zh)))
             return carry
 
-        lax.fori_loop(1, 4, step, 0)
+        lax.fori_loop(0, 3, step, 0)
+
+    order = (fp, 2 - zh, 3 - 3 * zh)
+
+    def line_copy(m, owner, target, slot, own):
+        n = mats[m][0].shape[0]
+        if own:
+            src = src_of(m, pl.multiple_of(r * (n // 2), n // 2), n // 2, 0)
+        else:
+            src = piece(m, owner, r)
+        return remote(src, piece(m, owner, r), zs.at[m, slot], zr.at[m, owner], {"fs": target})
+
+    def end_to_end(target):
+        return (f - target) * (f - target) == 9
+
+    def z_bulk(m, fn, keep):
+        def one(target):
+            ok = keep(target)
+            if mats[m][3]:
+                ok = ok & jnp.logical_not(end_to_end(target))
+
+            @pl.when(ok)
+            def _():
+                fn(z_copy(m, target))
+
+        others(one)
+
+    middle = (f == 1) | (f == 2)
+
+    def across(m):
+        return remote(piece(m, fp, r), piece(m, fp, r), zs.at[m, f], zr.at[m, fp], {"fs": 3 - fp})
 
     for m in range(6):
         own_copy(m).start()
-    pl.semaphore_wait(barrier, 6)
-
-    def send_weights(*ms):
-        def one(target):
-            for m in ms:
-                z_copy(m, target).start()
-
-        others(one)
-
-    def pass_on(*ms):
-        def one(owner):
-            for m in ms:
-                z_arrived(m, owner)
-                x_copy(m, owner).start()
-
-        others(one)
+    with jax.named_scope("barrier"):
+        pl.semaphore_wait(barrier, 6)
+
+    def start(copy):
+        copy.start()
+
+    def send_weights(*ms, keep=lambda target: target >= 0):
+        for m in ms:
+            z_bulk(m, start, keep)
+
+    def pass_on(m, *which):
+        for k in which:
+            owner = order[k]
+            z_arrived(m, owner)
+            if mats[m][3] and k == 0:
+
+                @pl.when(middle)
+                def _():
+                    across(m).start()
+
+            x_copy(m, owner).start()
+
+    def bulk_up():
+        send_weights(2, 3, 4, keep=lambda target: target > f)
+
+    def bulk_down():
+        send_weights(2, 3, 4, keep=lambda target: target < f)
+
+    def relay(d):
+        for sign in (-1, 1):
+            owner = f + sign * d
+
+            @pl.when((owner >= 0) & (owner <= 3))
+            def _():
+                for m in (0, 1):
+                    z_arrived(m, owner)
+                    after = f - sign
+
+                    @pl.when((after >= 0) & (after <= 3))
+                    def _():
+                        line_copy(m, owner, after, owner, False).start()
+
+                    x_copy(m, owner).start()
+
+        pl.when(f == d)(bulk_up)
+        pl.when(3 - f == d)(bulk_down)
 
     def collect(*ms):
         def one(owner):
@@ -254,12 +315,21 @@
         for m in ms:
             own_copy(m).wait()
 
-    send_weights(0, 1)
-    send_weights(2)
-    send_weights(3)
+    @pl.when(f < 3)
+    def _():
+        for m in (0, 1):
+            line_copy(m, f, f + 1, 4, True).start()
+
+    @pl.when(f > 0)
+    def _():
+        for m in (0, 1):
+            line_copy(m, f, f - 1, 5, True).start()
+
+    pl.when(f == 0)(bulk_up)
+    pl.when(f == 3)(bulk_down)
 
     def norm_rows(src, dst, gain_ref, count):
-        gain = gain_ref[...].astype(F32)
+        gain = gain_ref[...].astype(F32).reshape(1, width)
 
         def step(i, carry):
             at = pl.ds(pl.multiple_of(i * 16, 16), 16)
@@ -271,12 +341,18 @@
         lax.fori_loop(0, count // 16, step, 0, unroll=4)
 
     glu[pl.ds(0, 32), :] = jnp.zeros((32, cw), F32)
-    for j in range(4):
-        tok_copy(j).wait()
-    norm_rows(tok, normed, mix_gain, length)
-
-    pass_on(0, 1)
-    collect(0, 1)
+    for k in range(mix_taps.shape[0]):
+        tapb[pl.ds(8 * k, 8), :] = jnp.broadcast_to(mix_taps[k : k + 1, :].astype(F32), (8, mix_taps.shape[1]))
+    with jax.named_scope("tokwait"):
+        for j in range(4):
+            tok_copy(j).wait()
+        norm_rows(tok, normed, mix_gain, length)
+
+    with jax.named_scope("pass01"):
+        for d in (1, 2, 3):
+            relay(d)
+    with jax.named_scope("coll01"):
+        collect(0, 1)
 
     def head_cols(who):
         return pl.ds(pl.multiple_of(who * cw, 128), cw)
@@ -290,7 +366,9 @@
         remote(block, block, hs.at[kind, j], hr.at[kind, j], to_sib).wait_recv()
 
     reach = mix_taps.shape[0]
-    sub = 32
+    sub = 64
+
+    hgain = head_gain[...].astype(F32).reshape(1, cw)
 
     def mix_chunk(j, carry):
         both = jnp.dot(normed[rows(j), :], wpair[...], preferred_element_type=F32)
@@ -298,18 +376,23 @@
 
         def conv_step(i, inner):
             base = pl.multiple_of(j * chunk + i * sub, sub)
-            window = glu[pl.ds(base, sub + 32), :]
             acc = None
-            for k in range(reach):
-                o = 32 - (reach - 1) + k
-                term = window[o : o + sub, :] * mix_taps[k : k + 1, :].astype(F32)
-                acc = term if acc is None else acc + term
+            for e in range(8):
+                rot = None
+                for o in range(e, 33, 8):
+                    k = o - (33 - reach)
+                    if 0 <= k < reach:
+                        view = glu[pl.ds(base + 8 * (o // 8), sub + 8), :].reshape(sub // 8 + 1, 8, cw)
+                        term = view * tapb[pl.ds(8 * k, 8), :][None]
+                        rot = term if rot is None else rot + term
+                part_sum = rot.reshape(sub + 8, cw)[e : e + sub, :]
+                acc = part_sum if acc is None else acc + part_sum
             parts = []
             for h in range(0, cw, HEAD):
                 v = acc[:, h : h + HEAD]
                 v = v - jnp.mean(v, axis=-1, keepdims=True)
                 s = lax.rsqrt(jnp.mean(v * v, axis=-1, keepdims=True) + norm_floor)
-                v = v * s * head_gain[:, h : h + HEAD].astype(F32)
+                v = v * s * hgain[:, h : h + HEAD]
                 parts.append(v * jax.nn.sigmoid(v))
             heads[pl.ds(base, sub), head_cols(t)] = jnp.concatenate(parts, axis=1).astype(BF16)
             return inner
@@ -319,16 +402,21 @@
         head_send(1, j, t, to_y).start()
         return carry
 
-    lax.fori_loop(0, 4, mix_chunk, 0)
-    pass_on(2)
+    with jax.named_scope("mix"):
+        lax.fori_loop(0, 4, mix_chunk, 0)
+    with jax.named_scope("pass2"):
+        pass_on(2, 0, 1, 2)
+        pass_on(3, 0)
 
     def heads_on(j, carry):
         head_wait(1, j, ynb)
         head_send(2, j, ynb, to_sib).start()
         return carry
 
-    lax.fori_loop(0, 4, heads_on, 0)
-    collect(2)
+    with jax.named_scope("heads_on"):
+        lax.fori_loop(0, 4, heads_on, 0)
+    with jax.named_scope("coll2"):
+        collect(2)
 
     def hid_block(seq, j, who):
         return hid.at[seq, rows(j), pl.ds(pl.multiple_of(who * ow, 128), ow)]
@@ -349,34 +437,43 @@
         hid[zl, rows(j), pl.ds(pl.multiple_of(t * ow, 128), ow)] = total.astype(BF16)
         hid_send(0, j, zl, t, to_sib).start()
         hid_send(1, j, zl, t, to_y).start()
-        hid_send(2, j, zl, t, to_z).start()
+
+        @pl.when(jnp.logical_not(middle))
+        def _():
+            hid_send(2, j, zl, t, to_z).start()
+
         return carry
 
-    lax.fori_loop(0, 4, out_chunk, 0)
-    send_weights(4)
-    send_weights(5)
-
-    def hid_on(j, carry):
+    with jax.named_scope("outmm"):
+        lax.fori_loop(0, 4, out_chunk, 0)
+    with jax.named_scope("pass34a"):
+        pass_on(4, 0)
+        pass_on(3, 1)
+
+    def hid_own(j, carry):
         hid_wait(1, j, zl, ynb)
         hid_send(3, j, zl, ynb, to_sib).start()
-        hid_wait(2, j, 1 - zl, t)
-        hid_send(4, j, 1 - zl, t, to_sib).start()
-        hid_send(5, j, 1 - zl, t, to_y).start()
         return carry
 
-    lax.fori_loop(0, 4, hid_on, 0)
-    pass_on(3)
-
-    def hid_on2(j, carry):
-        hid_wait(5, j, 1 - zl, ynb)
-        hid_send(6, j, 1 - zl, ynb, to_sib).start()
-        return carry
-
-    lax.fori_loop(0, 4, hid_on2, 0)
-    pass_on(4)
-    collect(3, 4)
+    with jax.named_scope("hid_own"):
+        lax.fori_loop(0, 4, hid_own, 0)
+    with jax.named_scope("pass4b"):
+        pass_on(4, 1)
+
+    @pl.when(middle)
+    def _():
+        for j in range(4):
+            hid_send(2, j, zl, t, to_z).start()
+
+    with jax.named_scope("pass34c"):
+        pass_on(3, 2)
+        pass_on(4, 2)
+    send_weights(5)
+    with jax.named_scope("coll34"):
+        collect(3, 4)
 
     freach = ff_taps.shape[0]
+    ftap = ff_taps[:, pl.ds(pl.multiple_of(zl * hw, 128), hw)].astype(F32)
     asub = 32
 
     def ffn_chunk(i, carry):
@@ -395,7 +492,6 @@
             hid_wait(6, j, 1 - zl, far)
 
         norm_rows(hid.at[seq, rows(j), :], xc, ffn_gain, chunk)
-        keep = jnp.where(j == 0, 0.0, 1.0)
         gbuf[pl.ds(0, 8), :] = gbuf[pl.ds(chunk, 8), :]
 
         @pl.when(j == 0)
@@ -411,24 +507,42 @@
             acc = None
             for k in range(freach):
                 o = 8 - (freach - 1) + k
-                term = window[o : o + asub, :] * ff_taps[k : k + 1, :].astype(F32)
+                term = window[o : o + asub, :] * ftap[k : k + 1, :]
                 acc = term if acc is None else acc + term
             v = acc * jax.nn.sigmoid(acc) * ubuf[pl.ds(base, asub), :]
             prod[pl.ds(pl.multiple_of(seq * length + j * chunk + base, asub), asub), :] = v.astype(BF16)
             return inner
 
         lax.fori_loop(0, chunk // asub, act, 0)
+
+        @pl.when(first)
+        def _():
+            hid_wait(2, j, 1 - zl, t)
+            hid_send(4, j, 1 - zl, t, to_sib).start()
+            hid_send(5, j, 1 - zl, t, to_y).start()
+
+        @pl.when((middle & (i == 3)) | (jnp.logical_not(middle) & (i == 7)))
+        def _():
+            pass_on(5, 0)
+
+        @pl.when((i >= 1) & (i <= 4))
+        def _():
+            hid_wait(5, i - 1, 1 - zl, ynb)
+            hid_send(6, i - 1, 1 - zl, ynb, to_sib).start()
+
         return carry
 
-    lax.fori_loop(0, 8, ffn_chunk, 0)
-
-    own_copy(5).wait()
+    with jax.named_scope("ffn"):
+        lax.fori_loop(0, 8, ffn_chunk, 0)
+
+    with jax.named_scope("own5"):
+        own_copy(5).wait()
     blocks = 8
 
     def place(i):
         late = i // 4
         k = i % 4
-        owner = jnp.where(late == 0, 2 * zh + k // 2, 2 * (1 - zh) + k % 2)
+        owner = jnp.where(late == 0, 2 * zh + k // 2, jnp.where(k % 2 == 0, 2 - zh, 3 - 3 * zh))
         flip = jnp.where(late == 0, k % 2, k // 2)
         half = jnp.where(flip == 0, r, 1 - r)
         return owner, flip, half
@@ -436,21 +550,38 @@
     def q1(i):
         return remote(part.at[i % 3, 1 - c], rs1.at[i], qs.at[0, i], qr.at[0, i], to_sib)
 
-    def q2(i):
-        return remote(sum1.at[i % 3, 1 - y], rs2.at[i], qs.at[1, i], qr.at[1, i], to_y)
-
-    def q3(i):
-        return remote(sum2.at[i % 3, 1 - zl], rs3.at[i], qs.at[2, i], qr.at[2, i], to_z)
+    def q2(i, fn):
+        slot = i
+
+        @pl.when(i % 2 == 0)
+        def _():
+            fn(remote(sum1.at[slot, 1 - y], rs2.at[i], qs.at[1, i], qr.at[1, i], to_y))
+
+        @pl.when(i % 2 == 1)
+        def _():
+            fn(remote(sum1.at[slot, :, 1 - zl], rs2.at[i], qs.at[1, i], qr.at[1, i], to_z))
+
+    def q3(i, fn):
+        slot = i
+
+        @pl.when(i % 2 == 0)
+        def _():
+            fn(remote(sum2.at[slot, 1 - zl], rs3.at[i], qs.at[2, i], qr.at[2, i], to_z))
+
+        @pl.when(i % 2 == 1)
+        def _():
+            fn(remote(sum2.at[slot, 1 - y], rs3.at[i], qs.at[2, i], qr.at[2, i], to_y))
+
+    def got(copy):
+        copy.wait_recv()
+
+    def sent(copy):
+        copy.wait_send()
 
     def turn(i, carry):
-        @pl.when(i == 0)
-        def _():
-            z_arrived(5, fp)
-            x_copy(5, fp).start()
-
         @pl.when((i == 2) | (i == 3))
         def _():
-            owner = 2 * (1 - zh) + i % 2
+            owner = jnp.where(i == 2, 2 - zh, 3 - 3 * zh)
             z_arrived(5, owner)
             x_copy(5, owner).start()
 
@@ -487,48 +618,78 @@
             n = i - 1
             q1(n).wait_recv()
 
-            @pl.when(n >= 3)
+            sum1[n] = (part[n % 3, c].astype(F32) + rs1[n].astype(F32)).astype(BF16)
+            q2(n, start)
+
+        @pl.when((i >= 3) & (i <= blocks + 2))
+        def _():
+            n = i - 3
+            q2(n, got)
+
+
+            @pl.when(n % 2 == 0)
             def _():
-                q2(n - 3).wait_send()
-
-            sum1[n % 3] = (part[n % 3, c].astype(F32) + rs1[n].astype(F32)).astype(BF16)
-            q2(n).start()
-
-        @pl.when((i >= 2) & (i <= blocks + 1))
-        def _():
-            n = i - 2
-            q2(n).wait_recv()
-
-            @pl.when(n >= 3)
+                sum2[n] = (sum1[n, y].astype(F32) + rs2[n].astype(F32)).astype(BF16)
+
+            @pl.when(n % 2 == 1)
             def _():
-                q3(n - 3).wait_send()
-
-            sum2[n % 3] = (sum1[n % 3, y].astype(F32) + rs2[n].astype(F32)).astype(BF16)
-            q3(n).start()
-
-        @pl.when(i >= 3)
-        def _():
-            n = i - 3
-            q3(n).wait_recv()
+                sum2[n] = (sum1[n, :, zl].astype(F32) + rs2[n].astype(F32)).astype(BF16)
+
+            q3(n, start)
+
+        @pl.when(i >= 5)
+        def _():
+            n = i - 5
+            q3(n, got)
+            mine = jnp.where(n % 2 == 0, zl, y)
             owner, flip, half = place(n)
             cols = pl.ds(pl.multiple_of(owner * 2 * feat + half * feat, feat), feat)
             base = hid[zl, pl.ds(pl.multiple_of(t * chunk, chunk), chunk), cols].astype(F32)
-            total = base + (sum2[n % 3, zl].astype(F32) + rs3[n].astype(F32))
+            total = base + (sum2[n, mine].astype(F32) + rs3[n].astype(F32))
             out[0, :, cols] = total.astype(BF16)
 
         return carry
 
-    lax.fori_loop(0, blocks + 3, turn, 0)
-
-    for n in range(blocks - 3, blocks):
-        q1(n).wait_send()
-        q2(n).wait_send()
-        q3(n).wait_send()
-
-    def drain(target):
+    with jax.named_scope("rs"):
+        lax.fori_loop(0, blocks + 5, turn, 0)
+
+    for n in range(blocks):
+        if n >= blocks - 3:
+            q1(n).wait_send()
+        q2(n, sent)
+        q3(n, sent)
+
+    for m in (2, 3, 4, 5):
+        z_bulk(m, sent, lambda target: target >= 0)
+    for m in (3, 4, 5):
+
+        @pl.when(middle)
+        def _():
+            across(m).wait_send()
+
+    @pl.when(f < 3)
+    def _():
+        for m in (0, 1):
+            line_copy(m, f, f + 1, 4, True).wait_send()
+
+    @pl.when(f > 0)
+    def _():
+        for m in (0, 1):
+            line_copy(m, f, f - 1, 5, True).wait_send()
+
+    for d in (1, 2, 3):
+        for sign in (-1, 1):
+            owner = f + sign * d
+            after = f - sign
+
+            @pl.when((owner >= 0) & (owner <= 3) & (after >= 0) & (after <= 3))
+            def _():
+                for m in (0, 1):
+                    line_copy(m, owner, after, owner, False).wait_send()
+
+    def drain(owner):
         for m in range(6):
-            z_copy(m, target).wait_send()
-            x_copy(m, target).wait_send()
+            x_copy(m, owner).wait_send()
 
     others(drain)
 
@@ -556,17 +717,16 @@
     hw = ffgate_w.shape[1] // 2
     chunk = length // 4
     feat = down_w.shape[0] // 2
-    zl = lax.axis_index("fs") % 2
-    taps = lax.dynamic_slice_in_dim(ff_taps, zl * hw, hw, 1)
     scratch = [
         pltpu.VMEM((length, width), BF16),
         pltpu.VMEM((length, width), BF16),
         pltpu.VMEM((fs * value_w.shape[0], 2 * cw), BF16),
         pltpu.VMEM((fs * out_w.shape[0], ow), BF16),
-        pltpu.VMEM((length + 32, cw), F32),
+        pltpu.VMEM((length + 40, cw), F32),
         pltpu.VMEM((length, 4 * cw), BF16),
         pltpu.VMEM((2, length, width), BF16),
         pltpu.VMEM((chunk, width), BF16),
+        pltpu.VMEM((8 * mix_taps.shape[0], cw), F32),
         pltpu.VMEM((fs * ffgate_w.shape[0], hw), BF16),
         pltpu.VMEM((fs * up_w.shape[0], hw), BF16),
         pltpu.VMEM((fs * down_w.shape[0], hw), BF16),
@@ -575,14 +735,14 @@
         pltpu.VMEM((2 * length, hw), BF16),
         pltpu.VMEM((3, 2, 2, 2, chunk, feat), BF16),
         pltpu.VMEM((8, 2, 2, chunk, feat), BF16),
-        pltpu.VMEM((3, 2, 2, chunk, feat), BF16),
+        pltpu.VMEM((8, 2, 2, chunk, feat), BF16),
         pltpu.VMEM((8, 2, chunk, feat), BF16),
-        pltpu.VMEM((3, 2, chunk, feat), BF16),
+        pltpu.VMEM((8, 2, chunk, feat), BF16),
         pltpu.VMEM((8, chunk, feat), BF16),
         pltpu.SemaphoreType.DMA((6,)),
         pltpu.SemaphoreType.DMA((4,)),
     ]
-    scratch += [pltpu.SemaphoreType.DMA((6, 4))] * 4
+    scratch += [pltpu.SemaphoreType.DMA((6, n)) for n in (6, 4, 4, 4)]
     scratch += [pltpu.SemaphoreType.DMA((3, 4))] * 2
     scratch += [pltpu.SemaphoreType.DMA((7, 4))] * 2
     scratch += [pltpu.SemaphoreType.DMA((3, 8))] * 2
@@ -600,16 +760,16 @@
         name="layer",
     )(
         tokens,
-        mix_gain[None],
+        mix_gain,
         value_w,
         gate_w,
         mix_taps,
-        head_gain[None],
+        head_gain,
         out_w,
-        ffn_gain[None],
+        ffn_gain,
         ffgate_w,
         up_w,
-        taps,
+        ff_taps,
         down_w,
     )
 

time: 279 us -> 208 us (0.75)
  the two profiles are of different devices: /device:TPU:0 before, /device:TPU:16 now
where the time goes in v1:
time: 208 us; the launch traced here: 207 us
  Pallas kernels  205 us (99%)
  local copies, waits for them, and re-layouts  2.3 us (1%)
    pallas_call x1, Pallas kernels, fused(): pl.pallas_call(kernel, out_shape=jax.ShapeDtypeStruct((1, chunk, width),...  205 us

profile of v1, /device:TPU:16, one launch (start us, length us, event | category | flops | bytes accessed | tf_op | source)
XLA Modules:
  0.0 207.4 jit_solution(5928653180392315787)
XLA Ops:
  0.0 205.1 %layer.1 = bf16[1,256,2048]{2,1,0:T(8,128)(2,1)} custom-call(bf16[1,1024,2048]{2,1,0:T(8,128)(2,1)} %tokens.1, bf16[2048]{0:T(1024)(128)(2,1)} %mix_gain.1, bf16[512,256]{1,0:T(8,128)(2,1)} %value_w.1, bf16[512,256]{1,0:T(8,128)(2,1)} %gate_w.1, bf16[31,256]{1,0:T(8,128)(2,1)} %mix_taps.1, bf16[256]{0:T(256)(128)(2,1)} %head_gain.1, bf16[256,512]{1,0:T(8,128)(2,1)} %out_w.1, ...), custom_call_target="tpu_custom_call" | custom-call | tf_op jit(solution)/shard_map/layer/pallas_call | solution.py:751
  205.1 2.3 %copy.14 = bf16[1,256,2048]{2,1,0:T(8,128)(2,1)} copy(bf16[1,256,2048]{2,1,0:T(8,128)(2,1)} %layer.1) | data formatting | bytes 2097152

commit v2 on v1

--- a/solution.py
+++ b/solution.py
@@ -108,7 +108,6 @@
     glu,
     heads,
     hid,
-    xc,
     tapb,
     wg,
     wu,
@@ -147,7 +146,7 @@
     chunk = length // 4
     cw = value_w.shape[1]
     ow = out_w.shape[1]
-    hw = wg.shape[1]
+    hw = wg.shape[2]
     feat = down_w.shape[0] // 2
 
     def remote(src, dst, ss, rs, where):
@@ -168,57 +167,75 @@
     for j in range(4):
         tok_copy(j).start()
 
+    middle = (f == 1) | (f == 2)
+    shares = jnp.where(middle, 2, 1)
     mats = (
         (value_w, wpair, 0, False),
         (gate_w, wpair, cw, False),
         (out_w, wout, 0, False),
         (ffgate_w, wg, 0, True),
         (up_w, wu, 0, True),
-        (down_w, wd, 0, True),
+        (down_w, wd, None, True),
     )
 
-    def src_of(m, row, count, parity):
-        w, dst, col, halves = mats[m]
-        if halves:
-            return w.at[pl.ds(row, count), pl.ds(pl.multiple_of(parity * hw, 128), hw)]
+    def is_middle(plane):
+        return (plane == 1) | (plane == 2)
+
+    def src_of(m, row, count, plane, share):
+        w, dst, col, cut = mats[m]
+        if cut:
+            part_of = jnp.where(is_middle(plane), 1 + share, 0)
+            return w.at[pl.ds(row, count), pl.ds(pl.multiple_of(part_of * hw, 128), hw)]
         return w.at[pl.ds(row, count), :]
 
-    def dst_of(m, row, count):
-        w, dst, col, halves = mats[m]
-        size = hw if halves else w.shape[1]
-        return dst.at[pl.ds(row, count), pl.ds(col, size)]
-
-    def piece(m, owner, half):
+    def dst_of(m, row, count, share):
+        w, dst, col, cut = mats[m]
+        if cut and col is None:
+            return dst.at[pl.ds(row, count), pl.ds(share * hw, hw)]
+        if cut:
+            return dst.at[share, pl.ds(row, count), :]
+        return dst.at[pl.ds(row, count), pl.ds(col, w.shape[1])]
+
+    def piece(m, owner, half, share=0):
         n = mats[m][0].shape[0]
-        return dst_of(m, pl.multiple_of(owner * n + half * (n // 2), n // 2), n // 2)
-
-    def own_copy(m):
+        return dst_of(m, pl.multiple_of(owner * n + half * (n // 2), n // 2), n // 2, share)
+
+    def each_share(m, fn, plane=None):
+        fn(0)
+        if mats[m][3]:
+            two = middle if plane is None else is_middle(plane)
+
+            @pl.when(two)
+            def _():
+                fn(1)
+
+    def own_copy(m, share):
         n = mats[m][0].shape[0]
         return pltpu.make_async_copy(
-            src_of(m, 0, n, zl), dst_of(m, pl.multiple_of(f * n, n), n), loc.at[m]
+            src_of(m, 0, n, f, share), dst_of(m, pl.multiple_of(f * n, n), n, share), loc.at[m, share]
         )
 
-    def z_copy(m, target):
+    def z_copy(m, target, share):
         n = mats[m][0].shape[0]
         return remote(
-            src_of(m, pl.multiple_of(r * (n // 2), n // 2), n // 2, target % 2),
-            piece(m, f, r),
-            zs.at[m, target],
-            zr.at[m, f],
+            src_of(m, pl.multiple_of(r * (n // 2), n // 2), n // 2, target, share),
+            piece(m, f, r, share),
+            zs.at[m, target, share],
+            zr.at[m, f, share],
             {"fs": target},
         )
 
-    def z_arrived(m, owner):
-        n = mats[m][0].shape[0]
-        remote(piece(m, owner, r), piece(m, owner, r), zs.at[m, owner], zr.at[m, owner], to_x).wait_recv()
-
-    def x_copy(m, owner):
-        return remote(piece(m, owner, r), piece(m, owner, r), xs.at[m, owner], xr.at[m, owner], to_x)
-
-    def x_arrived(m, owner):
-        remote(
-            piece(m, owner, 1 - r), piece(m, owner, 1 - r), xs.at[m, owner], xr.at[m, owner], to_x
-        ).wait_recv()
+    def z_arrived(m, owner, share=0):
+        block = piece(m, owner, r, share)
+        remote(block, block, zs.at[m, owner, share], zr.at[m, owner, share], to_x).wait_recv()
+
+    def x_copy(m, owner, share=0):
+        block = piece(m, owner, r, share)
+        return remote(block, block, xs.at[m, owner, share], xr.at[m, owner, share], to_x)
+
+    def x_arrived(m, owner, share=0):
+        block = piece(m, owner, 1 - r, share)
+        remote(block, block, xs.at[m, owner, share], xr.at[m, owner, share], to_x).wait_recv()
 
     def others(fn):
         def step(k, carry):
@@ -232,60 +249,56 @@
     def line_copy(m, owner, target, slot, own):
         n = mats[m][0].shape[0]
         if own:
-            src = src_of(m, pl.multiple_of(r * (n // 2), n // 2), n // 2, 0)
+            src = src_of(m, pl.multiple_of(r * (n // 2), n // 2), n // 2, target, 0)
         else:
             src = piece(m, owner, r)
-        return remote(src, piece(m, owner, r), zs.at[m, slot], zr.at[m, owner], {"fs": target})
-
-    def end_to_end(target):
-        return (f - target) * (f - target) == 9
-
-    def z_bulk(m, fn, keep):
+        return remote(src, piece(m, owner, r), zs.at[m, slot, 0], zr.at[m, owner, 0], {"fs": target})
+
+    def z_bulk(m, fn, keep, shares_of=(0, 1)):
         def one(target):
             ok = keep(target)
             if mats[m][3]:
-                ok = ok & jnp.logical_not(end_to_end(target))
-
-            @pl.when(ok)
-            def _():
-                fn(z_copy(m, target))
+                ok = ok & (middle | (target != order[1]))
+
+            for share in shares_of:
+                if share == 1 and not mats[m][3]:
+                    continue
+                has = ok & is_middle(target) if share == 1 else ok
+
+                @pl.when(has)
+                def _():
+                    fn(z_copy(m, target, share))
 
         others(one)
 
-    middle = (f == 1) | (f == 2)
-
-    def across(m):
-        return remote(piece(m, fp, r), piece(m, fp, r), zs.at[m, f], zr.at[m, fp], {"fs": 3 - fp})
+    def across(m, share):
+        block = piece(m, fp, r, share)
+        return remote(block, block, zs.at[m, f, share], zr.at[m, fp, share], {"fs": 3 - f})
 
     for m in range(6):
-        own_copy(m).start()
+        each_share(m, lambda share: own_copy(m, share).start())
     with jax.named_scope("barrier"):
         pl.semaphore_wait(barrier, 6)
 
     def start(copy):
         copy.start()
 
-    def send_weights(*ms, keep=lambda target: target >= 0):
-        for m in ms:
-            z_bulk(m, start, keep)
-
-    def pass_on(m, *which):
-        for k in which:
-            owner = order[k]
-            z_arrived(m, owner)
-            if mats[m][3] and k == 0:
-
-                @pl.when(middle)
-                def _():
-                    across(m).start()
-
-            x_copy(m, owner).start()
-
-    def bulk_up():
-        send_weights(2, 3, 4, keep=lambda target: target > f)
-
-    def bulk_down():
-        send_weights(2, 3, 4, keep=lambda target: target < f)
+    def every(target):
+        return target >= 0
+
+    def ends_only(target):
+        return jnp.logical_not(is_middle(target))
+
+    def pass_on(m, k, share):
+        owner = order[k]
+        z_arrived(m, owner, share)
+        if mats[m][3] and k == 0:
+
+            @pl.when(middle)
+            def _():
+                across(m, share).start()
+
+        x_copy(m, owner, share).start()
 
     def relay(d):
         for sign in (-1, 1):
@@ -303,17 +316,15 @@
 
                     x_copy(m, owner).start()
 
-        pl.when(f == d)(bulk_up)
-        pl.when(3 - f == d)(bulk_down)
-
-    def collect(*ms):
+
+    def collect(share, *ms):
         def one(owner):
             for m in ms:
-                x_arrived(m, owner)
+                x_arrived(m, owner, share)
 
         others(one)
         for m in ms:
-            own_copy(m).wait()
+            own_copy(m, share).wait()
 
     @pl.when(f < 3)
     def _():
@@ -325,8 +336,10 @@
         for m in (0, 1):
             line_copy(m, f, f - 1, 5, True).start()
 
-    pl.when(f == 0)(bulk_up)
-    pl.when(f == 3)(bulk_down)
+    @pl.when(jnp.logical_not(middle))
+    def _():
+        for m in (3, 4):
+            z_bulk(m, start, is_middle, (0,))
 
     def norm_rows(src, dst, gain_ref, count):
         gain = gain_ref[...].astype(F32).reshape(1, width)
@@ -352,7 +365,19 @@
         for d in (1, 2, 3):
             relay(d)
     with jax.named_scope("coll01"):
-        collect(0, 1)
+        collect(0, 0, 1)
+    z_bulk(2, start, every)
+
+    @pl.when(middle)
+    def _():
+        for m in (3, 4):
+            z_bulk(m, start, is_middle, (0,))
+
+    @pl.when(jnp.logical_not(middle))
+    def _():
+        for m in (3, 4):
+            z_bulk(m, start, every, (1,))
+
 
     def head_cols(who):
         return pl.ds(pl.multiple_of(who * cw, 128), cw)
@@ -405,8 +430,13 @@
     with jax.named_scope("mix"):
         lax.fori_loop(0, 4, mix_chunk, 0)
     with jax.named_scope("pass2"):
-        pass_on(2, 0, 1, 2)
-        pass_on(3, 0)
+        for k in (0, 1, 2):
+            pass_on(2, k, 0)
+
+        @pl.when(middle)
+        def _():
+            for m in (3, 4):
+                pass_on(m, 0, 0)
 
     def heads_on(j, carry):
         head_wait(1, j, ynb)
@@ -416,7 +446,7 @@
     with jax.named_scope("heads_on"):
         lax.fori_loop(0, 4, heads_on, 0)
     with jax.named_scope("coll2"):
-        collect(2)
+        collect(0, 2)
 
     def hid_block(seq, j, who):
         return hid.at[seq, rows(j), pl.ds(pl.multiple_of(who * ow, 128), ow)]
@@ -446,60 +476,93 @@
 
     with jax.named_scope("outmm"):
         lax.fori_loop(0, 4, out_chunk, 0)
-    with jax.named_scope("pass34a"):
-        pass_on(4, 0)
-        pass_on(3, 1)
-
-    def hid_own(j, carry):
-        hid_wait(1, j, zl, ynb)
-        hid_send(3, j, zl, ynb, to_sib).start()
-        return carry
-
-    with jax.named_scope("hid_own"):
-        lax.fori_loop(0, 4, hid_own, 0)
-    with jax.named_scope("pass4b"):
-        pass_on(4, 1)
+
+    for m in (3, 4):
+        z_bulk(m, start, ends_only, (0,))
 
     @pl.when(middle)
     def _():
         for j in range(4):
             hid_send(2, j, zl, t, to_z).start()
-
-    with jax.named_scope("pass34c"):
-        pass_on(3, 2)
-        pass_on(4, 2)
-    send_weights(5)
-    with jax.named_scope("coll34"):
-        collect(3, 4)
+        for m in (3, 4):
+            z_bulk(m, start, every, (1,))
+
+    @pl.when(jnp.logical_not(middle))
+    def _():
+        z_bulk(5, start, is_middle)
+
+    with jax.named_scope("pass1"):
+
+        @pl.when(middle)
+        def _():
+            for m in (3, 4):
+                pass_on(m, 1, 0)
+
+    def hid_own(j, carry):
+        hid_wait(1, j, zl, ynb)
+        hid_send(3, j, zl, ynb, to_sib).start()
+
+        @pl.when(middle & (j == 2))
+        def _():
+            for m in (3, 4):
+                pass_on(m, 2, 0)
+
+        @pl.when(jnp.logical_not(middle) & (j == 2))
+        def _():
+            for m in (3, 4):
+                pass_on(m, 0, 0)
+
+        return carry
+
+    with jax.named_scope("hid_own"):
+        lax.fori_loop(0, 4, hid_own, 0)
+
+    with jax.named_scope("passE"):
+
+        @pl.when(jnp.logical_not(middle))
+        def _():
+            for k in (1, 2):
+                for m in (3, 4):
+                    pass_on(m, k, 0)
+
+    with jax.named_scope("pass0s1"):
+
+        @pl.when(middle)
+        def _():
+            for m in (3, 4):
+                pass_on(m, 0, 1)
+            z_bulk(5, start, is_middle)
+
+    def hid_partner(j, carry):
+        hid_wait(2, j, 1 - zl, t)
+        hid_send(4, j, 1 - zl, t, to_sib).start()
+        hid_send(5, j, 1 - zl, t, to_y).start()
+        return carry
+
+    with jax.named_scope("hid_partner"):
+        lax.fori_loop(0, 4, hid_partner, 0)
+    with jax.named_scope("collect"):
+        collect(0, 3, 4)
 
     freach = ff_taps.shape[0]
-    ftap = ff_taps[:, pl.ds(pl.multiple_of(zl * hw, 128), hw)].astype(F32)
     asub = 32
 
-    def ffn_chunk(i, carry):
-        first = i < 4
-        j = i % 4
-        seq = jnp.where(first, zl, 1 - zl)
-
-        @pl.when(first)
-        def _():
-            hid_wait(0, j, zl, sib)
-            hid_wait(3, j, zl, far)
-
-        @pl.when(jnp.logical_not(first))
-        def _():
-            hid_wait(4, j, 1 - zl, sib)
-            hid_wait(6, j, 1 - zl, far)
-
-        norm_rows(hid.at[seq, rows(j), :], xc, ffn_gain, chunk)
+    def ffn_rows(share, mine, j):
+        seq = zl if mine else 1 - zl
+        kept = normed if mine else tok
+        if share == 0:
+            norm_rows(hid.at[seq, rows(j), :], kept.at[rows(j), :], ffn_gain, chunk)
+        xc = kept[rows(j), :]
+        part_of = jnp.where(middle, 1 + share, 0)
+        ftap = ff_taps[:, pl.ds(pl.multiple_of(part_of * hw, 128), hw)].astype(F32)
         gbuf[pl.ds(0, 8), :] = gbuf[pl.ds(chunk, 8), :]
 
         @pl.when(j == 0)
         def _():
             gbuf[pl.ds(0, 8), :] = jnp.zeros((8, hw), F32)
 
-        gbuf[pl.ds(8, chunk), :] = jnp.dot(xc[...], wg[...], preferred_element_type=F32)
-        ubuf[...] = jnp.dot(xc[...], wu[...], preferred_element_type=F32)
+        gbuf[pl.ds(8, chunk), :] = jnp.dot(xc, wg[share], preferred_element_type=F32)
+        ubuf[...] = jnp.dot(xc, wu[share], preferred_element_type=F32)
 
         def act(a, inner):
             base = pl.multiple_of(a * asub, asub)
@@ -510,39 +573,79 @@
                 term = window[o : o + asub, :] * ftap[k : k + 1, :]
                 acc = term if acc is None else acc + term
             v = acc * jax.nn.sigmoid(acc) * ubuf[pl.ds(base, asub), :]
-            prod[pl.ds(pl.multiple_of(seq * length + j * chunk + base, asub), asub), :] = v.astype(BF16)
+            row = (4 * (j % 2) + 2 * (j // 2) + seq) * chunk + base
+            prod[pl.ds(pl.multiple_of(row, asub), asub), share * hw : (share + 1) * hw] = v.astype(BF16)
             return inner
 
         lax.fori_loop(0, chunk // asub, act, 0)
 
-        @pl.when(first)
-        def _():
-            hid_wait(2, j, 1 - zl, t)
-            hid_send(4, j, 1 - zl, t, to_sib).start()
-            hid_send(5, j, 1 - zl, t, to_y).start()
-
-        @pl.when((middle & (i == 3)) | (jnp.logical_not(middle) & (i == 7)))
-        def _():
-            pass_on(5, 0)
-
-        @pl.when((i >= 1) & (i <= 4))
-        def _():
-            hid_wait(5, i - 1, 1 - zl, ynb)
-            hid_send(6, i - 1, 1 - zl, ynb, to_sib).start()
+    def ffn_own(j, carry):
+        hid_wait(0, j, zl, sib)
+        hid_wait(3, j, zl, far)
+        ffn_rows(0, True, j)
+
+        @pl.when(middle & (j == 3))
+        def _():
+            for m in (3, 4):
+                pass_on(m, 1, 1)
+
+        @pl.when(j >= 1)
+        def _():
+            hid_wait(5, j - 1, 1 - zl, ynb)
+            hid_send(6, j - 1, 1 - zl, ynb, to_sib).start()
 
         return carry
 
-    with jax.named_scope("ffn"):
-        lax.fori_loop(0, 8, ffn_chunk, 0)
+    def ffn_partner(j, carry):
+        @pl.when(j == 0)
+        def _():
+            hid_wait(5, 3, 1 - zl, ynb)
+            hid_send(6, 3, 1 - zl, ynb, to_sib).start()
+
+        hid_wait(4, j, 1 - zl, sib)
+        hid_wait(6, j, 1 - zl, far)
+        ffn_rows(0, False, j)
+
+        @pl.when(middle & (j == 3))
+        def _():
+            for m in (3, 4):
+                pass_on(m, 2, 1)
+
+        return carry
+
+    with jax.named_scope("ffn1"):
+        lax.fori_loop(0, 4, ffn_own, 0)
+        z_bulk(5, start, ends_only, (0,))
+        lax.fori_loop(0, 4, ffn_partner, 0)
+
+    def pass_down(k):
+        each_share(5, lambda share: pass_on(5, k, share))
+
+    def ffn_second(mine, k, j, carry):
+        ffn_rows(1, mine, j)
+
+        @pl.when(j == 0)
+        def _():
+            pass_down(k)
+
+        return carry
+
+    with jax.named_scope("ffn2"):
+
+        @pl.when(middle)
+        def _():
+            collect(1, 3, 4)
+            lax.fori_loop(0, 4, functools.partial(ffn_second, True, 0), 0)
+            lax.fori_loop(0, 4, functools.partial(ffn_second, False, 1), 0)
 
     with jax.named_scope("own5"):
-        own_copy(5).wait()
+        each_share(5, lambda share: own_copy(5, share).wait())
     blocks = 8
 
     def place(i):
         late = i // 4
         k = i % 4
-        owner = jnp.where(late == 0, 2 * zh + k // 2, jnp.where(k % 2 == 0, 2 - zh, 3 - 3 * zh))
+        owner = jnp.where(late == 0, jnp.where(k < 2, 3 * zh, 1 + zh), jnp.where(k % 2 == 0, 2 - zh, 3 - 3 * zh))
         flip = jnp.where(late == 0, k % 2, k // 2)
         half = jnp.where(flip == 0, r, 1 - r)
         return owner, flip, half
@@ -579,11 +682,14 @@
         copy.wait_send()
 
     def turn(i, carry):
-        @pl.when((i == 2) | (i == 3))
-        def _():
-            owner = jnp.where(i == 2, 2 - zh, 3 - 3 * zh)
-            z_arrived(5, owner)
-            x_copy(5, owner).start()
+        @pl.when((i == 1) & jnp.logical_not(middle))
+        def _():
+            pass_down(0)
+            pass_down(1)
+
+        @pl.when(i == 3)
+        def _():
+            pass_down(2)
 
         @pl.when(i < blocks)
         def _():
@@ -591,7 +697,7 @@
 
             @pl.when((owner != f) & (flip == 1))
             def _():
-                x_arrived(5, owner)
+                each_share(5, lambda share: x_arrived(5, owner, share))
 
             @pl.when(i >= 3)
             def _():
@@ -599,26 +705,34 @@
 
             at = pl.ds(pl.multiple_of(owner * 2 * feat + half * feat, feat), feat)
 
-            def block_rows(b, inner):
-                cc, yy, ss = b // 4, (b // 2) % 2, b % 2
-                row = pl.multiple_of(ss * length + (2 * yy + cc) * chunk, chunk)
-                part[i % 3, cc, yy, ss] = lax.dot_general(
-                    prod[pl.ds(row, chunk), :],
-                    wd[at, :],
+            def down(cc, units):
+                return lax.dot_general(
+                    prod[pl.ds(pl.multiple_of(cc * 4 * chunk, chunk), 4 * chunk), :units],
+                    wd[at, :units],
                     (((1,), (1,)), ((), ())),
                     preferred_element_type=F32,
                 ).astype(BF16)
-                return inner
-
-            lax.fori_loop(0, 8, block_rows, 0)
+
+            def down_rows(cc):
+                @pl.when(middle)
+                def _():
+                    part[i % 3, cc] = down(cc, 2 * hw)
+
+                @pl.when(jnp.logical_not(middle))
+                def _():
+                    part[i % 3, cc] = down(cc, hw)
+
+            down_rows(1 - c)
             q1(i).start()
+            down_rows(c)
 
         @pl.when((i >= 1) & (i <= blocks))
         def _():
             n = i - 1
             q1(n).wait_recv()
 
-            sum1[n] = (part[n % 3, c].astype(F32) + rs1[n].astype(F32)).astype(BF16)
+            total = (part[n % 3, c].astype(F32) + rs1[n].astype(F32)).astype(BF16)
+            sum1[n] = total.reshape(2, 2, chunk, feat)
             q2(n, start)
 
         @pl.when((i >= 3) & (i <= blocks + 2))
@@ -660,12 +774,12 @@
         q3(n, sent)
 
     for m in (2, 3, 4, 5):
-        z_bulk(m, sent, lambda target: target >= 0)
+        z_bulk(m, sent, every)
     for m in (3, 4, 5):
 
         @pl.when(middle)
         def _():
-            across(m).wait_send()
+            each_share(m, lambda share: across(m, share).wait_send())
 
     @pl.when(f < 3)
     def _():
@@ -689,7 +803,7 @@
 
     def drain(owner):
         for m in range(6):
-            x_copy(m, owner).wait_send()
+            each_share(m, lambda share: x_copy(m, owner, share).wait_send())
 
     others(drain)
 
@@ -714,7 +828,7 @@
     _, length, width = tokens.shape
     fs = lax.axis_size("fs")
     cw, ow = value_w.shape[1], out_w.shape[1]
-    hw = ffgate_w.shape[1] // 2
+    hw = ffgate_w.shape[1] // 3
     chunk = length // 4
     feat = down_w.shape[0] // 2
     scratch = [
@@ -725,24 +839,23 @@
         pltpu.VMEM((length + 40, cw), F32),
         pltpu.VMEM((length, 4 * cw), BF16),
         pltpu.VMEM((2, length, width), BF16),
-        pltpu.VMEM((chunk, width), BF16),
         pltpu.VMEM((8 * mix_taps.shape[0], cw), F32),
-        pltpu.VMEM((fs * ffgate_w.shape[0], hw), BF16),
-        pltpu.VMEM((fs * up_w.shape[0], hw), BF16),
-        pltpu.VMEM((fs * down_w.shape[0], hw), BF16),
+        pltpu.VMEM((2, fs * ffgate_w.shape[0], hw), BF16),
+        pltpu.VMEM((2, fs * up_w.shape[0], hw), BF16),
+        pltpu.VMEM((fs * down_w.shape[0], 2 * hw), BF16),
         pltpu.VMEM((chunk + 8, hw), F32),
         pltpu.VMEM((chunk, hw), F32),
-        pltpu.VMEM((2 * length, hw), BF16),
-        pltpu.VMEM((3, 2, 2, 2, chunk, feat), BF16),
-        pltpu.VMEM((8, 2, 2, chunk, feat), BF16),
+        pltpu.VMEM((2 * length, 2 * hw), BF16),
+        pltpu.VMEM((3, 2, 4 * chunk, feat), BF16),
+        pltpu.VMEM((8, 4 * chunk, feat), BF16),
         pltpu.VMEM((8, 2, 2, chunk, feat), BF16),
         pltpu.VMEM((8, 2, chunk, feat), BF16),
         pltpu.VMEM((8, 2, chunk, feat), BF16),
         pltpu.VMEM((8, chunk, feat), BF16),
-        pltpu.SemaphoreType.DMA((6,)),
+        pltpu.SemaphoreType.DMA((6, 2)),
         pltpu.SemaphoreType.DMA((4,)),
     ]
-    scratch += [pltpu.SemaphoreType.DMA((6, n)) for n in (6, 4, 4, 4)]
+    scratch += [pltpu.SemaphoreType.DMA((6, n, 2)) for n in (6, 4, 4, 4)]
     scratch += [pltpu.SemaphoreType.DMA((3, 4))] * 2
     scratch += [pltpu.SemaphoreType.DMA((7, 4))] * 2
     scratch += [pltpu.SemaphoreType.DMA((3, 8))] * 2

time: 208 us -> 184 us (0.88)
  the two profiles are of different devices: /device:TPU:16 before, /device:TPU:0 now
where the time goes in v2:
time: 184 us; the launch traced here: 183 us
  Pallas kernels  181 us (98%)
  local copies, waits for them, and re-layouts  2.3 us (1%)
    pallas_call x1, Pallas kernels, fused(): pl.pallas_call(kernel, out_shape=jax.ShapeDtypeStruct((1, chunk, width),...  181 us

profile of v2, /device:TPU:0, one launch (start us, length us, event | category | flops | bytes accessed | tf_op | source)
XLA Modules:
  0.0 183.3 jit_solution(5224412676492495126)
XLA Ops:
  0.0 180.9 %layer.1 = bf16[1,256,2048]{2,1,0:T(8,128)(2,1)} custom-call(bf16[1,1024,2048]{2,1,0:T(8,128)(2,1)} %tokens.1, bf16[2048]{0:T(1024)(128)(2,1)} %mix_gain.1, bf16[512,256]{1,0:T(8,128)(2,1)} %value_w.1, bf16[512,256]{1,0:T(8,128)(2,1)} %gate_w.1, bf16[31,256]{1,0:T(8,128)(2,1)} %mix_taps.1, bf16[256]{0:T(256)(128)(2,1)} %head_gain.1, bf16[256,512]{1,0:T(8,128)(2,1)} %out_w.1, ...), custom_call_target="tpu_custom_call" | custom-call | tf_op jit(solution)/shard_map/layer/pallas_call | solution.py:864
  181.0 2.3 %copy.14 = bf16[1,256,2048]{2,1,0:T(8,128)(2,1)} copy(bf16[1,256,2048]{2,1,0:T(8,128)(2,1)} %layer.1) | data formatting | bytes 2097152

commit v3 on v2

--- a/solution.py
+++ b/solution.py
@@ -113,7 +113,6 @@
     wu,
     wd,
     gbuf,
-    ubuf,
     prod,
     part,
     rs1,
@@ -121,6 +120,8 @@
     rs2,
     sum2,
     rs3,
+    outv,
+    osem,
     loc,
     tsem,
     zs,
@@ -364,14 +365,14 @@
     with jax.named_scope("pass01"):
         for d in (1, 2, 3):
             relay(d)
-    with jax.named_scope("coll01"):
-        collect(0, 0, 1)
-    z_bulk(2, start, every)
-
     @pl.when(middle)
     def _():
         for m in (3, 4):
             z_bulk(m, start, is_middle, (0,))
+
+    with jax.named_scope("coll01"):
+        collect(0, 0, 1)
+    z_bulk(2, start, every)
 
     @pl.when(jnp.logical_not(middle))
     def _():
@@ -438,6 +439,11 @@
             for m in (3, 4):
                 pass_on(m, 0, 0)
 
+    @pl.when(middle)
+    def _():
+        for m in (3, 4):
+            z_bulk(m, start, lambda target: target == fp, (0,))
+
     def heads_on(j, carry):
         head_wait(1, j, ynb)
         head_send(2, j, ynb, to_sib).start()
@@ -478,7 +484,7 @@
         lax.fori_loop(0, 4, out_chunk, 0)
 
     for m in (3, 4):
-        z_bulk(m, start, ends_only, (0,))
+        z_bulk(m, start, lambda target: ends_only(target) & (target != fp), (0,))
 
     @pl.when(middle)
     def _():
@@ -498,6 +504,11 @@
             for m in (3, 4):
                 pass_on(m, 1, 0)
 
+        @pl.when(jnp.logical_not(middle))
+        def _():
+            for m in (3, 4):
+                pass_on(m, 0, 0)
+
     def hid_own(j, carry):
         hid_wait(1, j, zl, ynb)
         hid_send(3, j, zl, ynb, to_sib).start()
@@ -506,11 +517,6 @@
         def _():
             for m in (3, 4):
                 pass_on(m, 2, 0)
-
-        @pl.when(jnp.logical_not(middle) & (j == 2))
-        def _():
-            for m in (3, 4):
-                pass_on(m, 0, 0)
 
         return carry
 
@@ -539,20 +545,21 @@
         hid_send(5, j, 1 - zl, t, to_y).start()
         return carry
 
-    with jax.named_scope("hid_partner"):
-        lax.fori_loop(0, 4, hid_partner, 0)
-    with jax.named_scope("collect"):
-        collect(0, 3, 4)
-
     freach = ff_taps.shape[0]
     asub = 32
 
-    def ffn_rows(share, mine, j):
+    def kept_rows(mine, j):
+        return (normed if mine else tok)[rows(j), :]
+
+    def prod_row(mine, j):
         seq = zl if mine else 1 - zl
-        kept = normed if mine else tok
+        return pl.multiple_of((4 * (j % 2) + 2 * (j // 2) + seq) * chunk, chunk)
+
+    def gate_rows(share, mine, j):
         if share == 0:
+            kept = normed if mine else tok
+            seq = zl if mine else 1 - zl
             norm_rows(hid.at[seq, rows(j), :], kept.at[rows(j), :], ffn_gain, chunk)
-        xc = kept[rows(j), :]
         part_of = jnp.where(middle, 1 + share, 0)
         ftap = ff_taps[:, pl.ds(pl.multiple_of(part_of * hw, 128), hw)].astype(F32)
         gbuf[pl.ds(0, 8), :] = gbuf[pl.ds(chunk, 8), :]
@@ -561,8 +568,7 @@
         def _():
             gbuf[pl.ds(0, 8), :] = jnp.zeros((8, hw), F32)
 
-        gbuf[pl.ds(8, chunk), :] = jnp.dot(xc, wg[share], preferred_element_type=F32)
-        ubuf[...] = jnp.dot(xc, wu[share], preferred_element_type=F32)
+        gbuf[pl.ds(8, chunk), :] = jnp.dot(kept_rows(mine, j), wg[share], preferred_element_type=F32)
 
         def act(a, inner):
             base = pl.multiple_of(a * asub, asub)
@@ -572,71 +578,116 @@
                 o = 8 - (freach - 1) + k
                 term = window[o : o + asub, :] * ftap[k : k + 1, :]
                 acc = term if acc is None else acc + term
-            v = acc * jax.nn.sigmoid(acc) * ubuf[pl.ds(base, asub), :]
-            row = (4 * (j % 2) + 2 * (j // 2) + seq) * chunk + base
-            prod[pl.ds(pl.multiple_of(row, asub), asub), share * hw : (share + 1) * hw] = v.astype(BF16)
+            gated = (acc * jax.nn.sigmoid(acc)).astype(BF16)
+            prod[pl.ds(prod_row(mine, j) + base, asub), share * hw : (share + 1) * hw] = gated
             return inner
 
         lax.fori_loop(0, chunk // asub, act, 0)
 
-    def ffn_own(j, carry):
+    def up_rows(share, mine, j):
+        at = pl.ds(prod_row(mine, j), chunk)
+        cols = slice(share * hw, (share + 1) * hw)
+        ff_up = jnp.dot(kept_rows(mine, j), wu[share], preferred_element_type=F32)
+        prod[at, cols] = (prod[at, cols].astype(F32) * ff_up).astype(BF16)
+
+    def pass_down(k):
+        each_share(5, lambda share: pass_on(5, k, share))
+
+    def hid_last(j):
+        hid_wait(5, j, 1 - zl, ynb)
+        hid_send(6, j, 1 - zl, ynb, to_sib).start()
+
+    def own_ready(j):
         hid_wait(0, j, zl, sib)
         hid_wait(3, j, zl, far)
-        ffn_rows(0, True, j)
-
-        @pl.when(middle & (j == 3))
-        def _():
+
+    def partner_ready(j):
+        hid_wait(4, j, 1 - zl, sib)
+        hid_wait(6, j, 1 - zl, far)
+
+    def four(fn):
+        def step(j, carry):
+            fn(j)
+            return carry
+
+        lax.fori_loop(0, 4, step, 0)
+
+    @pl.when(middle)
+    def _():
+        with jax.named_scope("hid_partner"):
+            lax.fori_loop(0, 4, hid_partner, 0)
+        with jax.named_scope("collect"):
+            collect(0, 3, 4)
+
+        def own(j):
+            own_ready(j)
+            gate_rows(0, True, j)
+            up_rows(0, True, j)
+            pl.when(j >= 1)(lambda: hid_last(j - 1))
+
+        def partner(j):
+            pl.when(j == 0)(lambda: hid_last(3))
+            partner_ready(j)
+            gate_rows(0, False, j)
+            up_rows(0, False, j)
+
+        with jax.named_scope("ffn1"):
+            four(own)
             for m in (3, 4):
                 pass_on(m, 1, 1)
-
-        @pl.when(j >= 1)
-        def _():
-            hid_wait(5, j - 1, 1 - zl, ynb)
-            hid_send(6, j - 1, 1 - zl, ynb, to_sib).start()
-
-        return carry
-
-    def ffn_partner(j, carry):
-        @pl.when(j == 0)
-        def _():
-            hid_wait(5, 3, 1 - zl, ynb)
-            hid_send(6, 3, 1 - zl, ynb, to_sib).start()
-
-        hid_wait(4, j, 1 - zl, sib)
-        hid_wait(6, j, 1 - zl, far)
-        ffn_rows(0, False, j)
-
-        @pl.when(middle & (j == 3))
-        def _():
-            for m in (3, 4):
-                pass_on(m, 2, 1)
-
-        return carry
-
-    with jax.named_scope("ffn1"):
-        lax.fori_loop(0, 4, ffn_own, 0)
-        z_bulk(5, start, ends_only, (0,))
-        lax.fori_loop(0, 4, ffn_partner, 0)
-
-    def pass_down(k):
-        each_share(5, lambda share: pass_on(5, k, share))
-
-    def ffn_second(mine, k, j, carry):
-        ffn_rows(1, mine, j)
-
-        @pl.when(j == 0)
-        def _():
-            pass_down(k)
-
-        return carry
-
-    with jax.named_scope("ffn2"):
-
-        @pl.when(middle)
-        def _():
-            collect(1, 3, 4)
-            lax.fori_loop(0, 4, functools.partial(ffn_second, True, 0), 0)
-            lax.fori_loop(0, 4, functools.partial(ffn_second, False, 1), 0)
+            z_bulk(5, start, ends_only, (0,))
+            four(partner)
+        with jax.named_scope("coll1g"):
+            pass_on(3, 2, 1)
+            collect(1, 3)
+
+        def own_gate(j):
+            gate_rows(1, True, j)
+            pl.when(j == 1)(lambda: pass_on(4, 2, 1))
+
+        with jax.named_scope("gate2"):
+            four(own_gate)
+            pass_down(0)
+            four(lambda j: gate_rows(1, False, j))
+        with jax.named_scope("coll1u"):
+            collect(1, 4)
+        with jax.named_scope("up2"):
+            four(lambda j: up_rows(1, True, j))
+            pass_down(1)
+            four(lambda j: up_rows(1, False, j))
+
+    @pl.when(jnp.logical_not(middle))
+    def _():
+        with jax.named_scope("hid_partner"):
+            lax.fori_loop(0, 2, hid_partner, 0)
+        with jax.named_scope("collect"):
+            collect(0, 3)
+
+        def own_gate(j):
+            own_ready(j)
+            gate_rows(0, True, j)
+            pl.when(j < 2)(lambda: hid_partner(j + 2, None))
+            pl.when(j == 2)(lambda: hid_last(0))
+
+        with jax.named_scope("gate1"):
+            four(own_gate)
+        with jax.named_scope("coll0u"):
+            collect(0, 4)
+            z_bulk(5, start, ends_only, (0,))
+
+        def partner(j):
+            partner_ready(j)
+            gate_rows(0, False, j)
+            up_rows(0, False, j)
+            pl.when(j == 0)(lambda: hid_last(3))
+            pl.when(j == 2)(lambda: pass_down(0))
+
+        with jax.named_scope("up1"):
+            four(lambda j: up_rows(0, True, j))
+            hid_last(1)
+            hid_last(2)
+        with jax.named_scope("ffnp"):
+            four(partner)
 
     with jax.named_scope("own5"):
         each_share(5, lambda share: own_copy(5, share).wait())
@@ -645,8 +696,10 @@
     def place(i):
         late = i // 4
         k = i % 4
-        owner = jnp.where(late == 0, jnp.where(k < 2, 3 * zh, 1 + zh), jnp.where(k % 2 == 0, 2 - zh, 3 - 3 * zh))
-        flip = jnp.where(late == 0, k % 2, k // 2)
+        flip = k // 2
+        early_owner = jnp.where(k % 2 == 0, 3 * zh, 1 + zh)
+        late_owner = jnp.where(k % 2 == 0, 2 - zh, 3 - 3 * zh)
+        owner = jnp.where(late == 0, early_owner, late_owner)
         half = jnp.where(flip == 0, r, 1 - r)
         return owner, flip, half
 
@@ -656,22 +709,22 @@
     def q2(i, fn):
         slot = i
 
+        @pl.when(i % 2 == 1)
+        def _():
+            fn(remote(sum1.at[slot, 1 - y], rs2.at[i], qs.at[1, i], qr.at[1, i], to_y))
+
         @pl.when(i % 2 == 0)
-        def _():
-            fn(remote(sum1.at[slot, 1 - y], rs2.at[i], qs.at[1, i], qr.at[1, i], to_y))
-
-        @pl.when(i % 2 == 1)
         def _():
             fn(remote(sum1.at[slot, :, 1 - zl], rs2.at[i], qs.at[1, i], qr.at[1, i], to_z))
 
     def q3(i, fn):
         slot = i
 
+        @pl.when(i % 2 == 1)
+        def _():
+            fn(remote(sum2.at[slot, 1 - zl], rs3.at[i], qs.at[2, i], qr.at[2, i], to_z))
+
         @pl.when(i % 2 == 0)
-        def _():
-            fn(remote(sum2.at[slot, 1 - zl], rs3.at[i], qs.at[2, i], qr.at[2, i], to_z))
-
-        @pl.when(i % 2 == 1)
         def _():
             fn(remote(sum2.at[slot, 1 - y], rs3.at[i], qs.at[2, i], qr.at[2, i], to_y))
 
@@ -681,10 +734,73 @@
     def sent(copy):
         copy.wait_send()
 
+    def drain_weights(*ms):
+        for m in ms:
+            if m >= 2:
+                z_bulk(m, sent, every)
+            if m >= 3:
+
+                @pl.when(middle)
+                def _():
+                    each_share(m, lambda share: across(m, share).wait_send())
+
+        def passed(owner):
+            for m in ms:
+                each_share(m, lambda share: x_copy(m, owner, share).wait_send())
+
+        others(passed)
+
+    def drain_early():
+        drain_weights(0, 1, 2, 3, 4)
+
+        @pl.when(f < 3)
+        def _():
+            for m in (0, 1):
+                line_copy(m, f, f + 1, 4, True).wait_send()
+
+        @pl.when(f > 0)
+        def _():
+            for m in (0, 1):
+                line_copy(m, f, f - 1, 5, True).wait_send()
+
+        for d in (1, 2, 3):
+            for sign in (-1, 1):
+                owner = f + sign * d
+                after = f - sign
+
+                @pl.when((owner >= 0) & (owner <= 3) & (after >= 0) & (after <= 3))
+                def _():
+                    for m in (0, 1):
+                        line_copy(m, owner, after, owner, False).wait_send()
+
+        def drain_chunks(j, carry):
+            head_send(0, j, t, to_sib).wait_send()
+            head_send(1, j, t, to_y).wait_send()
+            head_send(2, j, ynb, to_sib).wait_send()
+            hid_send(0, j, zl, t, to_sib).wait_send()
+            hid_send(1, j, zl, t, to_y).wait_send()
+            hid_send(2, j, zl, t, to_z).wait_send()
+            hid_send(3, j, zl, ynb, to_sib).wait_send()
+            hid_send(4, j, 1 - zl, t, to_sib).wait_send()
+            hid_send(5, j, 1 - zl, t, to_y).wait_send()
+            hid_send(6, j, 1 - zl, ynb, to_sib).wait_send()
+            return carry
+
+        lax.fori_loop(0, 4, drain_chunks, 0)
+
+    def out_cols(n):
+        owner, flip, half = place(n)
+        return pl.ds(pl.multiple_of(owner * 2 * feat + half * feat, feat), feat)
+
+    def out_copy(n):
+        cols = out_cols(n)
+        return pltpu.make_async_copy(outv.at[:, cols], out.at[0, :, cols], osem.at[n])
+
     def turn(i, carry):
+        pl.when(i == 6)(drain_early)
+
         @pl.when((i == 1) & jnp.logical_not(middle))
         def _():
-            pass_down(0)
             pass_down(1)
 
         @pl.when(i == 3)
@@ -741,12 +857,12 @@
             q2(n, got)
 
 
+            @pl.when(n % 2 == 1)
+            def _():
+                sum2[n] = (sum1[n, y].astype(F32) + rs2[n].astype(F32)).astype(BF16)
+
             @pl.when(n % 2 == 0)
             def _():
-                sum2[n] = (sum1[n, y].astype(F32) + rs2[n].astype(F32)).astype(BF16)
-
-            @pl.when(n % 2 == 1)
-            def _():
                 sum2[n] = (sum1[n, :, zl].astype(F32) + rs2[n].astype(F32)).astype(BF16)
 
             q3(n, start)
@@ -755,12 +871,12 @@
         def _():
             n = i - 5
             q3(n, got)
-            mine = jnp.where(n % 2 == 0, zl, y)
-            owner, flip, half = place(n)
-            cols = pl.ds(pl.multiple_of(owner * 2 * feat + half * feat, feat), feat)
+            mine = jnp.where(n % 2 == 1, zl, y)
+            cols = out_cols(n)
             base = hid[zl, pl.ds(pl.multiple_of(t * chunk, chunk), chunk), cols].astype(F32)
             total = base + (sum2[n, mine].astype(F32) + rs3[n].astype(F32))
-            out[0, :, cols] = total.astype(BF16)
+            outv[:, cols] = total.astype(BF16)
+            out_copy(n).start()
 
         return carry
 
@@ -773,54 +889,10 @@
         q2(n, sent)
         q3(n, sent)
 
-    for m in (2, 3, 4, 5):
-        z_bulk(m, sent, every)
-    for m in (3, 4, 5):
-
-        @pl.when(middle)
-        def _():
-            each_share(m, lambda share: across(m, share).wait_send())
-
-    @pl.when(f < 3)
-    def _():
-        for m in (0, 1):
-            line_copy(m, f, f + 1, 4, True).wait_send()
-
-    @pl.when(f > 0)
-    def _():
-        for m in (0, 1):
-            line_copy(m, f, f - 1, 5, True).wait_send()
-
-    for d in (1, 2, 3):
-        for sign in (-1, 1):
-            owner = f + sign * d
-            after = f - sign
-
-            @pl.when((owner >= 0) & (owner <= 3) & (after >= 0) & (after <= 3))
-            def _():
-                for m in (0, 1):
-                    line_copy(m, owner, after, owner, False).wait_send()
-
-    def drain(owner):
-        for m in range(6):
-            each_share(m, lambda share: x_copy(m, owner, share).wait_send())
-
-    others(drain)
-
-    def drain_chunks(j, carry):
-        head_send(0, j, t, to_sib).wait_send()
-        head_send(1, j, t, to_y).wait_send()
-        head_send(2, j, ynb, to_sib).wait_send()
-        hid_send(0, j, zl, t, to_sib).wait_send()
-        hid_send(1, j, zl, t, to_y).wait_send()
-        hid_send(2, j, zl, t, to_z).wait_send()
-        hid_send(3, j, zl, ynb, to_sib).wait_send()
-        hid_send(4, j, 1 - zl, t, to_sib).wait_send()
-        hid_send(5, j, 1 - zl, t, to_y).wait_send()
-        hid_send(6, j, 1 - zl, ynb, to_sib).wait_send()
-        return carry
-
-    lax.fori_loop(0, 4, drain_chunks, 0)
+    with jax.named_scope("drain"):
+        drain_weights(5)
+        for n in range(blocks):
+            out_copy(n).wait()
 
 
 def fused(*arrays):
@@ -844,7 +916,6 @@
         pltpu.VMEM((2, fs * up_w.shape[0], hw), BF16),
         pltpu.VMEM((fs * down_w.shape[0], 2 * hw), BF16),
         pltpu.VMEM((chunk + 8, hw), F32),
-        pltpu.VMEM((chunk, hw), F32),
         pltpu.VMEM((2 * length, 2 * hw), BF16),
         pltpu.VMEM((3, 2, 4 * chunk, feat), BF16),
         pltpu.VMEM((8, 4 * chunk, feat), BF16),
@@ -852,6 +923,8 @@
         pltpu.VMEM((8, 2, chunk, feat), BF16),
         pltpu.VMEM((8, 2, chunk, feat), BF16),
         pltpu.VMEM((8, chunk, feat), BF16),
+        pltpu.VMEM((chunk, width), BF16),
+        pltpu.SemaphoreType.DMA((8,)),
         pltpu.SemaphoreType.DMA((6, 2)),
         pltpu.SemaphoreType.DMA((4,)),
     ]
@@ -865,7 +938,7 @@
         kernel,
         out_shape=jax.ShapeDtypeStruct((1, chunk, width), BF16),
         in_specs=[anywhere, small, anywhere, anywhere, small, small, anywhere, small, anywhere, anywhere, small, anywhere],
-        out_specs=small,
+        out_specs=anywhere,
         scratch_shapes=scratch,
         compiler_params=pltpu.CompilerParams(
             collective_id=0, has_side_effects=True, vmem_limit_bytes=67043328

time: 184 us -> 176 us (0.957)
  Pallas kernels: 181 us -> 173 us
    pallas_call x1, Pallas kernels: 181 us -> 173 us  [fused(): pl.pallas_call(kernel, out_shape=jax.ShapeDtypeStruct((1, chunk, width),...]
where the time goes in v3:
time: 176 us; the launch traced here: 175 us
  Pallas kernels  173 us (98%)
  local copies, waits for them, and re-layouts  2.3 us (1%)
    pallas_call x1, Pallas kernels, fused(): pl.pallas_call(kernel, out_shape=jax.ShapeDtypeStruct((1, chunk, width),...  173 us

profile of v3, /device:TPU:0, one launch (start us, length us, event | category | flops | bytes accessed | tf_op | source)
XLA Modules:
  0.0 175.4 jit_solution(3498777037870404470)
XLA Ops:
  0.0 173.1 %layer.1 = bf16[1,256,2048]{2,1,0:T(8,128)(2,1)} custom-call(bf16[1,1024,2048]{2,1,0:T(8,128)(2,1)} %tokens.1, bf16[2048]{0:T(1024)(128)(2,1)} %mix_gain.1, bf16[512,256]{1,0:T(8,128)(2,1)} %value_w.1, bf16[512,256]{1,0:T(8,128)(2,1)} %gate_w.1, bf16[31,256]{1,0:T(8,128)(2,1)} %mix_taps.1, bf16[256]{0:T(256)(128)(2,1)} %head_gain.1, bf16[256,512]{1,0:T(8,128)(2,1)} %out_w.1, ...), custom_call_target="tpu_custom_call" | custom-call | tf_op jit(solution)/shard_map/layer/pallas_call | solution.py:937
  173.1 2.3 %copy.14 = bf16[1,256,2048]{2,1,0:T(8,128)(2,1)} copy(bf16[1,256,2048]{2,1,0:T(8,128)(2,1)} %layer.1) | data formatting | bytes 2097152

commit v4 on v3

--- a/solution.py
+++ b/solution.py
@@ -643,15 +643,15 @@
 
         def own_gate(j):
             gate_rows(1, True, j)
-            pl.when(j == 1)(lambda: pass_on(4, 2, 1))
+            pl.when(j == 0)(lambda: pass_on(4, 2, 1))
 
         with jax.named_scope("gate2"):
             four(own_gate)
-            pass_down(0)
             four(lambda j: gate_rows(1, False, j))
         with jax.named_scope("coll1u"):
             collect(1, 4)
         with jax.named_scope("up2"):
+            pass_down(0)
             four(lambda j: up_rows(1, True, j))
             pass_down(1)
             four(lambda j: up_rows(1, False, j))
@@ -842,18 +842,18 @@
             q1(i).start()
             down_rows(c)
 
-        @pl.when((i >= 1) & (i <= blocks))
-        def _():
-            n = i - 1
+        @pl.when(i < blocks)
+        def _():
+            n = i
             q1(n).wait_recv()
 
             total = (part[n % 3, c].astype(F32) + rs1[n].astype(F32)).astype(BF16)
             sum1[n] = total.reshape(2, 2, chunk, feat)
             q2(n, start)
 
-        @pl.when((i >= 3) & (i <= blocks + 2))
-        def _():
-            n = i - 3
+        @pl.when((i >= 2) & (i <= blocks + 1))
+        def _():
+            n = i - 2
             q2(n, got)
 
 
@@ -867,9 +867,9 @@
 
             q3(n, start)
 
-        @pl.when(i >= 5)
-        def _():
-            n = i - 5
+        @pl.when(i >= 4)
+        def _():
+            n = i - 4
             q3(n, got)
             mine = jnp.where(n % 2 == 1, zl, y)
             cols = out_cols(n)
@@ -881,7 +881,7 @@
         return carry
 
     with jax.named_scope("rs"):
-        lax.fori_loop(0, blocks + 5, turn, 0)
+        lax.fori_loop(0, blocks + 4, turn, 0)
 
     for n in range(blocks):
         if n >= blocks - 3:

time: 176 us -> 173 us (0.983)
  Pallas kernels: 173 us -> 171 us
    pallas_call x1, Pallas kernels: 173 us -> 171 us  [fused(): pl.pallas_call(kernel, out_shape=jax.ShapeDtypeStruct((1, chunk, width),...]
where the time goes in v4:
time: 173 us
  Pallas kernels  171 us (99%)
  local copies, waits for them, and re-layouts  2.3 us (1%)
    pallas_call x1, Pallas kernels, fused(): pl.pallas_call(kernel, out_shape=jax.ShapeDtypeStruct((1, chunk, width),...  171 us

profile of v4, /device:TPU:0, one launch (start us, length us, event | category | flops | bytes accessed | tf_op | source)
XLA Modules:
  0.0 173.0 jit_solution(14540019138115796304)
XLA Ops:
  0.0 170.7 %layer.1 = bf16[1,256,2048]{2,1,0:T(8,128)(2,1)} custom-call(bf16[1,1024,2048]{2,1,0:T(8,128)(2,1)} %tokens.1, bf16[2048]{0:T(1024)(128)(2,1)} %mix_gain.1, bf16[512,256]{1,0:T(8,128)(2,1)} %value_w.1, bf16[512,256]{1,0:T(8,128)(2,1)} %gate_w.1, bf16[31,256]{1,0:T(8,128)(2,1)} %mix_taps.1, bf16[256]{0:T(256)(128)(2,1)} %head_gain.1, bf16[256,512]{1,0:T(8,128)(2,1)} %out_w.1, ...), custom_call_target="tpu_custom_call" | custom-call | tf_op jit(solution)/shard_map/layer/pallas_call | solution.py:937
  170.7 2.3 %copy.14 = bf16[1,256,2048]{2,1,0:T(8,128)(2,1)} copy(bf16[1,256,2048]{2,1,0:T(8,128)(2,1)} %layer.1) | data formatting | bytes 2097152
